TPU v7x, 32 devices: a whole 2x2x4 slice. The times are simulated.
32 devices in a mesh: kv: 8 (over z, x), tp: 4 (over y, core).
Axes of the slice: x: 2, y: 2, z: 4, core: 2. Of those that a mesh axis runs over, the one named last changes fastest.
Arguments:
- hidden: bfloat16 [128, 4, 2048], P(None, None, 'kv'), may hold values from -18 to 18
- norm_gain: float32 [2048], replicated, may hold values from 0.1 to 1.9
- w_query: bfloat16 [2048, 1024], P(None, 'tp'), may hold values from -0.125 to 0.125
- w_forget: bfloat16 [2048, 1024], P(None, 'tp'), may hold values from -0.125 to 0.125
- w_input: bfloat16 [2048, 1024], P(None, 'tp'), may hold values from -0.125 to 0.125
- w_outgate: bfloat16 [2048, 1024], P(None, 'tp'), may hold values from -0.125 to 0.125
- w_out: bfloat16 [1024, 2048], replicated, may hold values from -0.1875 to 0.1875
- floor: float32 [1024], P('tp'), may hold values from 0 to 0.95
- head_gain: float32 [128], replicated, may hold values from 0.1 to 1.9
- base_state: float32 [128, 8, 128, 128], P('kv', 'tp'), may hold values from -4 to 4
- prev_forget: bfloat16 [128, 4, 1024], P('kv', None, 'tp'), may hold values from -6 to 6
- prev_input: bfloat16 [128, 4, 1024], P('kv', None, 'tp'), may hold values from -6 to 6
- accepted: int32 [128], P('kv'), may hold values from 0 to 4
Outputs:
- mixed: bfloat16 [128, 4, 2048], P(None, None, 'kv')
- taken_state: float32 [128, 8, 128, 128], P('kv', 'tp')
All inputs are finite; a program needn't handle non-finite values.
Results may differ from a plain program's by a relative error of at most 0.014.
Values may be sent and summed in bfloat16 or wider, within the bound.
No kernel may reach another device: no remote copies, remote signals or barrier semaphores. Data moves between devices by JAX's collectives and lax.ppermute only.
A program may use at most 64 MiB of HBM per device.

v0:
```python
import functools

import jax
import jax.numpy as jnp
from jax import lax
from jax.experimental import pallas as pl
from jax.experimental.pallas import tpu as pltpu
from jax.sharding import PartitionSpec as P

HEAD_DIM = 128
F32 = jnp.float32
BF16 = jnp.bfloat16


def state_kernel(seqs, props, heads, acc, floor, prev_forget, prev_input, base, taken, low, a_sc, b_sc, v_sc, s_sc, in_sem, out_sem):
    loads = [pltpu.make_async_copy(base.at[s], s_sc.at[s], in_sem.at[s]) for s in range(seqs)]
    for c in loads:
        c.start()
    fl = floor[...]
    row = lax.broadcasted_iota(jnp.int32, (seqs, seqs), 0)
    col = lax.broadcasted_iota(jnp.int32, (seqs, seqs), 1)
    count = jnp.sum(jnp.where(row == col, acc[...], 0), axis=1, keepdims=True)
    f, k = [], []
    for j in range(props):
        live = j < count
        fj = fl + (1.0 - fl) * jax.nn.sigmoid(prev_forget[j].astype(F32))
        f.append(jnp.where(live, fj, 1.0))
        k.append(jnp.where(live, 1.0 - fj, 0.0))
    tail = jnp.ones_like(f[0])
    b = [None] * props
    for j in reversed(range(props)):
        b[j] = k[j] * tail
        tail = tail * f[j]
    b = jnp.concatenate(b, axis=0)
    hi = b.astype(BF16).astype(F32)
    both = jnp.concatenate([hi, b - hi], axis=0)
    v = jnp.concatenate([prev_input[j].astype(F32) for j in range(props)] * 2, axis=0)
    owner = lax.broadcasted_iota(jnp.int32, (2 * props * seqs, HEAD_DIM), 0) % seqs
    for h in range(heads):
        cols = slice(h * HEAD_DIM, (h + 1) * HEAD_DIM)
        a_sc[h] = tail[:, cols].T
        b_sc[h] = both[:, cols].T.astype(BF16)
        v_sc[h] = v[:, cols]
    stores = []
    for s in range(seqs):
        loads[s].wait()
        for h in range(heads):
            own_v = jnp.where(owner == s, v_sc[h], 0.0).astype(BF16)
            add = jnp.dot(b_sc[h], own_v, preferred_element_type=F32)
            new = a_sc[h, :, s : s + 1] * s_sc[s, h] + add
            s_sc[s, h] = new
            low[s, h] = new.astype(BF16)
        c = pltpu.make_async_copy(s_sc.at[s], taken.at[s], out_sem.at[s])
        c.start()
        stores.append(c)
    for c in stores:
        c.wait()


def heads_kernel(
    n_kv, seqs, props, heads, x, gain, wq, wf, wi, wg, floor, head_gain, low, out,
    w_sc, s_sc, n_sc, q_sc, o_sc, w_sem, s_sem,
):
    rows = seqs * props
    loads = [pltpu.make_async_copy(w, w_sc.at[i], w_sem.at[i]) for i, w in enumerate((wf, wq, wi, wg))]
    for c in loads:
        c.start()
    s_load = pltpu.make_async_copy(low, s_sc, s_sem)
    s_load.start()
    width = x.shape[2]
    total = jnp.zeros((rows, 1), F32)
    for i in range(n_kv):
        xi = x[i].astype(F32)
        total = total + jnp.sum(xi * xi, axis=1, keepdims=True)
    scale = lax.rsqrt(total / (n_kv * width) + 1e-06)
    for i in range(n_kv):
        c = slice(i * width, (i + 1) * width)
        n_sc[:, c] = (x[i].astype(F32) * scale * gain[:, c]).astype(BF16)

    def project(i):
        loads[i].wait()
        y = jnp.dot(n_sc[...], w_sc[i], preferred_element_type=F32).astype(BF16).astype(F32)
        return [y[t * seqs : (t + 1) * seqs, :] for t in range(props)]

    fl = floor[...]
    f = [fl + (1.0 - fl) * jax.nn.sigmoid(y) for y in project(0)]
    q = [y * jax.nn.sigmoid(y) for y in project(1)]
    decay = jnp.ones_like(f[0])
    for t in range(props):
        decay = decay * f[t]
        qt = q[t] * decay
        for h in range(heads):
            at = (h * props + t) * seqs
            q_sc[at : at + seqs, :] = qt[:, h * HEAD_DIM : (h + 1) * HEAD_DIM]
    v = project(2)
    s_load.wait()
    for s in range(seqs):
        for h in range(heads):
            each = pl.ds(h * props * seqs + s, props, stride=seqs)
            lhs = q_sc[each, :].astype(BF16)
            o_sc[each, :] = jnp.dot(lhs, s_sc[s, h], preferred_element_type=F32)
    g = project(3)
    for t in range(props):
        parts = []
        for h in range(heads):
            cols = slice(h * HEAD_DIM, (h + 1) * HEAD_DIM)
            at = (h * props + t) * seqs
            o = o_sc[at : at + seqs, :]
            reach = q[t][:, cols]
            for i in reversed(range(t + 1)):
                score = jnp.sum(reach * (1.0 - f[i][:, cols]), axis=1, keepdims=True)
                o = o + score * v[i][:, cols]
                reach = reach * f[i][:, cols]
            norm = lax.rsqrt(jnp.mean(o * o, axis=1, keepdims=True) + 1e-05)
            gate = g[t][:, cols]
            parts.append(o * norm * head_gain[...] * (gate * jax.nn.sigmoid(gate)))
        out[t * seqs : (t + 1) * seqs, :] = jnp.concatenate(parts, axis=1).astype(BF16)


def out_kernel(n_tp, n_kv, x, w, out):
    own, feats = x.shape[2], out.shape[2]
    block = max(feats, 2 * HEAD_DIM)
    for b in range(n_kv * feats // block):
        cols = slice(b * block, (b + 1) * block)
        total = jnp.dot(x[0], w[:own, cols], preferred_element_type=F32)
        for i in range(1, n_tp):
            total = total + jnp.dot(x[i], w[i * own : (i + 1) * own, cols], preferred_element_type=F32)
        for i in range(block // feats):
            out[b * (block // feats) + i] = total[:, i * feats : (i + 1) * feats].astype(BF16)


def shards(
    n_kv, n_tp, hidden, norm_gain, w_query, w_forget, w_input, w_outgate, w_out, floor, head_gain,
    base_state, prev_forget, prev_input, accepted,
):
    all_seqs, props, feats = hidden.shape
    seqs = all_seqs // n_kv
    rows = seqs * props
    heads = w_query.shape[1] // HEAD_DIM
    own = heads * HEAD_DIM
    vmem, anym, hbm = (pl.BlockSpec(memory_space=m) for m in (pltpu.VMEM, pl.ANY, pltpu.HBM))

    arrived = lax.all_to_all(hidden, "kv", split_axis=0, concat_axis=0, tiled=True)
    x = arrived.reshape(n_kv, seqs, props, feats).transpose(0, 2, 1, 3).reshape(n_kv, rows, feats)

    floor_row = floor.reshape(1, own)
    state_shape = base_state.shape
    taken_state, low = pl.pallas_call(
        functools.partial(state_kernel, seqs, props, heads),
        out_shape=(jax.ShapeDtypeStruct(state_shape, F32), jax.ShapeDtypeStruct(state_shape, BF16)),
        in_specs=[vmem, vmem, vmem, vmem, hbm],
        out_specs=(hbm, vmem),
        scratch_shapes=[
            pltpu.VMEM((heads, HEAD_DIM, seqs), F32),
            pltpu.VMEM((heads, HEAD_DIM, 2 * rows), BF16),
            pltpu.VMEM((heads, 2 * rows, HEAD_DIM), F32),
            pltpu.VMEM(state_shape, F32),
            pltpu.SemaphoreType.DMA((seqs,)),
            pltpu.SemaphoreType.DMA((seqs,)),
        ],
        cost_estimate=pl.CostEstimate(flops=200_000_000, bytes_accessed=6_000_000, transcendentals=0),
        compiler_params=pltpu.CompilerParams(vmem_limit_bytes=16 * 2**20),
        name="state",
    )(
        accepted.reshape(1, seqs), floor_row, prev_forget.transpose(1, 0, 2), prev_input.transpose(1, 0, 2), base_state
    )

    mixed_heads = pl.pallas_call(
        functools.partial(heads_kernel, n_kv, seqs, props, heads),
        out_shape=jax.ShapeDtypeStruct((rows, own), BF16),
        in_specs=[vmem, vmem, anym, anym, hbm, hbm, vmem, vmem, anym],
        out_specs=vmem,
        scratch_shapes=[
            pltpu.VMEM((4, n_kv * feats, own), BF16),
            pltpu.VMEM(state_shape, BF16),
            pltpu.VMEM((rows, n_kv * feats), BF16),
            pltpu.VMEM((heads * rows, HEAD_DIM), F32),
            pltpu.VMEM((heads * rows, HEAD_DIM), F32),
            pltpu.SemaphoreType.DMA((4,)),
            pltpu.SemaphoreType.DMA,
        ],
        cost_estimate=pl.CostEstimate(flops=300_000_000, bytes_accessed=6_000_000, transcendentals=0),
        compiler_params=pltpu.CompilerParams(vmem_limit_bytes=16 * 2**20),
        name="heads",
    )(x, norm_gain.reshape(1, -1), w_query, w_forget, w_input, w_outgate, floor_row, head_gain.reshape(1, -1), low)

    whole = lax.all_gather(mixed_heads, "tp", axis=0)
    finished = pl.pallas_call(
        functools.partial(out_kernel, n_tp, n_kv),
        out_shape=jax.ShapeDtypeStruct((n_kv, rows, feats), BF16),
        in_specs=[vmem, vmem],
        out_specs=vmem,
        compiler_params=pltpu.CompilerParams(vmem_limit_bytes=16 * 2**20),
        name="out",
    )(whole, w_out)
    mixed = lax.all_to_all(finished, "kv", split_axis=0, concat_axis=0, tiled=True)
    mixed = mixed.reshape(n_kv, props, seqs, feats).transpose(0, 2, 1, 3).reshape(all_seqs, props, feats)
    return (mixed, taken_state)


def solution(mesh):
    placed = (
        P(None, None, "kv"),
        P(),
        P(None, "tp"),
        P(None, "tp"),
        P(None, "tp"),
        P(None, "tp"),
        P(),
        P("tp"),
        P(),
        P("kv", "tp", None, None),
        P("kv", None, "tp"),
        P("kv", None, "tp"),
        P("kv"),
    )
    return jax.shard_map(
        functools.partial(shards, mesh.shape["kv"], mesh.shape["tp"]),
        mesh=mesh,
        in_specs=placed,
        out_specs=(P(None, None, "kv"), P("kv", "tp", None, None)),
        check_vma=False,
    )
```

profile of v0, /device:TPU:0, one launch (start us, length us, event | category | flops | bytes accessed | tf_op | source)
XLA Modules:
  0.0 45.8 jit_solution(14037434323100313)
XLA Ops:
  0.6 0.0 copy-start.8
  0.6 0.0 copy-start.10
  0.7 0.0 copy-start.6
  0.7 7.4 %all-to-all-start = ((bf16[128,4,256]{2,1,0:T(4,128)(2,1)}), bf16[128,4,256]{2,1,0:T(4,128)(2,1)S(1)}, u32[]{:S(2)}, u32[]{:S(2)}) async-start(bf16[128,4,256]{2,1,0:T(4,128)(2,1)} %param.13), calls=%async_computation | async-start | bytes 524288 | tf_op jit(solution)/shard_map/all_to_all | solution.py:143
  8.1 0.8 %copy_bitcast_fusion = (bf16[4,16,256]{2,1,0:T(8,128)(2,1)S(1)}, bf16[4,16,256]{2,1,0:T(8,128)(2,1)S(1)}) fusion(bf16[16,4,256]{2,1,0:T(4,128)(2,1)} %param.24, bf16[16,4,256]{2,1,0:T(4,128)(2,1)} %param.23), kind=kLoop, calls=%fused_computation | loop fusion | bytes 131072 | tf_op jit(solution)/shard_map/transpose | solution.py:165
  8.9 0.0 copy-start.1
  8.9 1.6 %copy-done.1 = f32[16,2,128,128]{3,2,1,0:T(8,128)S(1)} copy-done((f32[16,2,128,128]{3,2,1,0:T(8,128)S(1)}, f32[16,2,128,128]{3,2,1,0:T(8,128)}, u32[]{:S(2)}) %copy-start.1) | copy-done | bytes 2097176
  10.5 0.0 copy-start.7
  10.5 0.7 %copy-done.7 = f32[256]{0:T(256)S(1)} copy-done((f32[256]{0:T(256)S(1)}, f32[256]{0:T(256)}, u32[]{:S(2)}) %copy-start.7) | copy-done | bytes 1048
  11.1 0.0 copy-start.9
  11.1 0.7 %copy-done.9 = s32[16]{0:T(128)S(1)} copy-done((s32[16]{0:T(128)S(1)}, s32[16]{0:T(128)}, u32[]{:S(2)}) %copy-start.9) | copy-done | bytes 88
  11.8 0.0 copy-start.2
  11.8 0.0 copy-start.3
  11.8 6.4 %state.1 = (f32[16,2,128,128]{3,2,1,0:T(8,128)}, bf16[16,2,128,128]{3,2,1,0:T(8,128)(2,1)S(1)}) custom-call(s32[1,16]{1,0:T(1,128)S(1)} %bitcast.22, f32[1,256]{1,0:T(1,128)S(1)} %bitcast.20, bf16[4,16,256]{2,1,0:T(8,128)(2,1)S(1)} %get-tuple-element.7.prev_forget, bf16[4,16,256]{2,1,0:T(8,128)(2,1)S(1)} %get-tuple-element.6.prev_input, ...), custom_call_target="tpu_custom_call" | custom-call | flops 200000000 | bytes 6000000 | tf_op jit(solution)/shard_map/state/pallas_call | solution.py:148
  18.2 0.0 all-to-all-done
  18.3 0.0 copy-done.8
  18.3 0.0 copy-done.10
  18.3 0.0 copy-done.6
  18.3 0.0 copy-done.2
  18.3 0.0 copy-done.3
  18.3 0.0 copy-start.4
  18.3 1.2 %copy-done.4 = bf16[2048,256]{1,0:T(8,128)(2,1)S(1)} copy-done((bf16[2048,256]{1,0:T(8,128)(2,1)S(1)}, bf16[2048,256]{1,0:T(8,128)(2,1)}, u32[]{:S(2)}) %copy-start.4) | copy-done | bytes 1048600
  19.5 0.0 copy-start.5
  19.6 1.2 %copy-done.5 = bf16[2048,256]{1,0:T(8,128)(2,1)S(1)} copy-done((bf16[2048,256]{1,0:T(8,128)(2,1)S(1)}, bf16[2048,256]{1,0:T(8,128)(2,1)}, u32[]{:S(2)}) %copy-start.5) | copy-done | bytes 1048600
  20.8 0.0 copy-start
  20.8 2.7 %heads.1 = bf16[64,256]{1,0:T(8,128)(2,1)S(1)} custom-call(bf16[8,64,256]{2,1,0:T(8,128)(2,1)S(1)} %bitcast.17, f32[1,2048]{1,0:T(1,128)S(1)} %bitcast.19, bf16[2048,256]{1,0:T(8,128)(2,1)S(1)} %copy-done.2, bf16[2048,256]{1,0:T(8,128)(2,1)S(1)} %copy-done.3, bf16[2048,256]{1,0:T(8,128)(2,1)S(1)} %copy-done.4, bf16[2048,256]{1,0:T(8,128)(2,1)S(1)} %copy-done.5, ...), custom_call_target="tpu_custom_call" | custom-call | flops 300000000 | bytes 6000000 | tf_op jit(solution)/shard_map/heads/pallas_call | solution.py:168
  23.5 5.4 %all-gather = bf16[256,256]{1,0:T(8,128)(2,1)S(1)} all-gather(bf16[64,256]{1,0:T(8,128)(2,1)S(1)} %heads.1), channel_id=2, replica_groups=mesh['kv'=8,'tp'=4] {'tp'}, dimensions={0}, use_global_device_ids=true | all-gather | bytes 163840 | tf_op jit(solution)/shard_map/all_gather | solution.py:187
  28.9 0.0 copy-done
  28.9 0.8 %out.1 = bf16[8,64,256]{2,1,0:T(8,128)(2,1)S(1)} custom-call(bf16[4,64,256]{2,1,0:T(8,128)(2,1)S(1)} %bitcast.18, bf16[1024,2048]{1,0:T(8,128)(2,1)S(1)} %copy-done), custom_call_target="tpu_custom_call" | custom-call | tf_op jit(solution)/shard_map/out/pallas_call | solution.py:188
  29.8 15.2 %all_to_all.10 = bf16[8,64,256]{2,1,0:T(8,128)(2,1)S(1)} all-to-all(bf16[8,64,256]{2,1,0:T(8,128)(2,1)S(1)} %out.1), channel_id=1, replica_groups=mesh['kv'=8,'tp'=4] {'kv'}, dimensions={0} | all-to-all | bytes 524288 | tf_op jit(solution)/shard_map/all_to_all | solution.py:196
  45.0 0.8 %copy.18 = bf16[8,16,4,256]{3,2,1,0:T(4,128)(2,1)} copy(bf16[8,16,4,256]{3,1,2,0:T(8,128)(2,1)S(1)} %bitcast.25) | data formatting | bytes 524288 | tf_op jit(solution)/shard_map/transpose | solution.py:197
  (1 shorter events, 0.0 us)
Async XLA Ops:
  0.6 17.6 %copy-start.8 = (f32[256]{0:T(256)S(1)}, f32[256]{0:T(256)}, u32[]{:S(2)}) copy-start(f32[256]{0:T(256)} %param.20) | copy-start | bytes 3076
  0.6 17.6 %copy-start.10 = (f32[128]{0:T(128)S(1)}, f32[128]{0:T(128)}, u32[]{:S(2)}) copy-start(f32[128]{0:T(128)} %param.21) | copy-start | bytes 1540
  0.7 17.6 %copy-start.6 = (f32[2048]{0:T(1024)S(1)}, f32[2048]{0:T(1024)}, u32[]{:S(2)}) copy-start(f32[2048]{0:T(1024)} %param.14) | copy-start | bytes 24580
  0.7 17.6 %all-to-all-start = ((bf16[128,4,256]{2,1,0:T(4,128)(2,1)}), bf16[128,4,256]{2,1,0:T(4,128)(2,1)S(1)}, u32[]{:S(2)}, u32[]{:S(2)}) async-start(bf16[128,4,256]{2,1,0:T(4,128)(2,1)} %param.13), calls=%async_computation | async-start | bytes 524288 | tf_op jit(solution)/shard_map/all_to_all | solution.py:143
  8.9 1.6 %copy-start.1 = (f32[16,2,128,128]{3,2,1,0:T(8,128)S(1)}, f32[16,2,128,128]{3,2,1,0:T(8,128)}, u32[]{:S(2)}) copy-start(f32[16,2,128,128]{3,2,1,0:T(8,128)} %base.1) | copy-start | bytes 6291460
  10.5 0.7 %copy-start.7 = (f32[256]{0:T(256)S(1)}, f32[256]{0:T(256)}, u32[]{:S(2)}) copy-start(f32[256]{0:T(256)} %param.20) | copy-start | bytes 3076
  11.1 0.7 %copy-start.9 = (s32[16]{0:T(128)S(1)}, s32[16]{0:T(128)}, u32[]{:S(2)}) copy-start(s32[16]{0:T(128)} %param.25) | copy-start | bytes 196
  11.8 6.5 %copy-start.2 = (bf16[2048,256]{1,0:T(8,128)(2,1)S(1)}, bf16[2048,256]{1,0:T(8,128)(2,1)}, u32[]{:S(2)}) copy-start(bf16[2048,256]{1,0:T(8,128)(2,1)} %wq.1) | copy-start | bytes 3145732
  11.8 6.5 %copy-start.3 = (bf16[2048,256]{1,0:T(8,128)(2,1)S(1)}, bf16[2048,256]{1,0:T(8,128)(2,1)}, u32[]{:S(2)}) copy-start(bf16[2048,256]{1,0:T(8,128)(2,1)} %wf.1) | copy-start | bytes 3145732
  18.3 1.2 %copy-start.4 = (bf16[2048,256]{1,0:T(8,128)(2,1)S(1)}, bf16[2048,256]{1,0:T(8,128)(2,1)}, u32[]{:S(2)}) copy-start(bf16[2048,256]{1,0:T(8,128)(2,1)} %wi.1) | copy-start | bytes 3145732
  19.5 1.2 %copy-start.5 = (bf16[2048,256]{1,0:T(8,128)(2,1)S(1)}, bf16[2048,256]{1,0:T(8,128)(2,1)}, u32[]{:S(2)}) copy-start(bf16[2048,256]{1,0:T(8,128)(2,1)} %wg.1) | copy-start | bytes 3145732
  20.8 8.1 %copy-start = (bf16[1024,2048]{1,0:T(8,128)(2,1)S(1)}, bf16[1024,2048]{1,0:T(8,128)(2,1)}, u32[]{:S(2)}) copy-start(bf16[1024,2048]{1,0:T(8,128)(2,1)} %w.1) | copy-start | bytes 12582916
where the time goes:
time: 46.3 us; the launch traced here: 45.8 us
  blocking collectives  20.6 us (44%)
  Pallas kernels  9.96 us (22%)
  starting transfers between devices  7.42 us (16%)
  local copies, waits for them, and re-layouts  7.04 us (15%)
  between operations  0.76 us (2%)
    all_to_all x1, blocking collectives, shards(): lax.all_to_all(finished, 'kv', split_axis=0, concat_axis=0, tiled=True)  15.2 us
    all_to_all x1, starting transfers between devices, shards(): lax.all_to_all(hidden, 'kv', split_axis=0, concat_axis=0, tiled=True)  7.42 us
    pallas_call x1, Pallas kernels, shards(): pl.pallas_call(functools.partial(state_kernel, seqs, props, heads), out_s...  6.41 us
    all_gather x1, blocking collectives, shards(): whole = lax.all_gather(mixed_heads, 'tp', axis=0)  5.42 us
    unnamed x22, local copies, waits for them, and re-layouts  5.39 us
    pallas_call x1, Pallas kernels, shards(): pl.pallas_call(functools.partial(heads_kernel, n_kv, seqs, props, heads),...  2.72 us
  transfers between devices with their start and end apart: 1, of which 0 were waited for; matrix products, arithmetic and copies ran while one was open for 2% of the time, Pallas kernels for 14%

commit v1 on v0

--- a/solution.py
+++ b/solution.py
@@ -143,6 +143,7 @@
     arrived = lax.all_to_all(hidden, "kv", split_axis=0, concat_axis=0, tiled=True)
     x = arrived.reshape(n_kv, seqs, props, feats).transpose(0, 2, 1, 3).reshape(n_kv, rows, feats)
 
+    base_state, w_input, w_outgate = (pltpu.with_memory_space_constraint(a, pltpu.HBM) for a in (base_state, w_input, w_outgate))
     floor_row = floor.reshape(1, own)
     state_shape = base_state.shape
     taken_state, low = pl.pallas_call(
@@ -162,7 +163,8 @@
         compiler_params=pltpu.CompilerParams(vmem_limit_bytes=16 * 2**20),
         name="state",
     )(
-        accepted.reshape(1, seqs), floor_row, prev_forget.transpose(1, 0, 2), prev_input.transpose(1, 0, 2), base_state
+        pltpu.with_memory_space_constraint(accepted.reshape(1, seqs), pltpu.HBM),
+        pltpu.with_memory_space_constraint(floor_row, pltpu.HBM), prev_forget.transpose(1, 0, 2), prev_input.transpose(1, 0, 2), base_state
     )
 
     mixed_heads = pl.pallas_call(

time: 46.3 us -> 40.4 us (0.87)
  local copies, waits for them, and re-layouts: 7.04 us -> 1.68 us
  waiting for transfers between devices: 0.01 us -> 3.02 us
  blocking collectives: 20.6 us -> 18.2 us
  Pallas kernels: 9.96 us -> 8.88 us
    unnamed x22 -> x12, local copies, waits for them, and re-layouts: 5.39 us -> 0.03 us
    all_to_all x1, waiting for transfers between devices: 0.01 us -> 3.02 us  [shards(): lax.all_to_all(hidden, 'kv', split_axis=0, concat_axis=0, tiled=True)]
    all_to_all x1, blocking collectives: 15.2 us -> 12.8 us  [shards(): lax.all_to_all(finished, 'kv', split_axis=0, concat_axis=0, tiled=True)]
    pallas_call x1, Pallas kernels: 6.41 us -> 5.1 us  [shards(): pl.pallas_call(functools.partial(state_kernel, seqs, props, heads), out_s...]
  transfers between devices with their start and end apart: 1 -> 1, of which waited for: 0 -> 1; matrix products, arithmetic and copies ran while one was open for 2% -> 2% of each run, Pallas kernels for 14% -> 13%
where the time goes in v1:
time: 40.4 us; the launch traced here: 40 us
  blocking collectives  18.2 us (45%)
  Pallas kernels  8.88 us (22%)
  starting transfers between devices  7.42 us (18%)
  waiting for transfers between devices  3.02 us (7%)
  local copies, waits for them, and re-layouts  1.68 us (4%)
  between operations  0.75 us (2%)
    all_to_all x1, blocking collectives, shards(): lax.all_to_all(finished, 'kv', split_axis=0, concat_axis=0, tiled=True)  12.8 us
    all_to_all x1, starting transfers between devices, shards(): lax.all_to_all(hidden, 'kv', split_axis=0, concat_axis=0, tiled=True)  7.42 us
    all_gather x1, blocking collectives, shards(): whole = lax.all_gather(mixed_heads, 'tp', axis=0)  5.42 us
    pallas_call x1, Pallas kernels, shards(): pl.pallas_call(functools.partial(state_kernel, seqs, props, heads), out_s...  5.1 us
    all_to_all x1, waiting for transfers between devices, shards(): lax.all_to_all(hidden, 'kv', split_axis=0, concat_axis=0, tiled=True)  3.02 us
    pallas_call x1, Pallas kernels, shards(): pl.pallas_call(functools.partial(heads_kernel, n_kv, seqs, props, heads),...  2.94 us
    transpose x1, local copies, waits for them, and re-layouts, shards(): mixed.reshape(n_kv, props, seqs, feats).transpose(0, 2, 1, 3)  0.84 us
    pallas_call x1, Pallas kernels, shards(): pl.pallas_call(functools.partial(out_kernel, n_tp, n_kv), out_shape=jax.S...  0.83 us
  transfers between devices with their start and end apart: 1, of which 1 were waited for; matrix products, arithmetic and copies ran while one was open for 2% of the time, Pallas kernels for 13%

profile of v1, /device:TPU:0, one launch (start us, length us, event | category | flops | bytes accessed | tf_op | source)
XLA Modules:
  0.0 40.0 jit_solution(5620249688606114444)
XLA Ops:
  0.6 0.0 copy-start.4
  0.6 0.0 copy-start.5
  0.7 0.0 copy-start.2
  0.7 0.0 copy-start.1
  0.7 0.0 copy-start.3
  0.7 7.4 %all-to-all-start = ((bf16[128,4,256]{2,1,0:T(4,128)(2,1)}), bf16[128,4,256]{2,1,0:T(4,128)(2,1)S(1)}, u32[]{:S(2)}, u32[]{:S(2)}) async-start(bf16[128,4,256]{2,1,0:T(4,128)(2,1)} %param.13), calls=%async_computation | async-start | bytes 524288 | tf_op jit(solution)/shard_map/all_to_all | solution.py:143
  8.1 0.8 %copy_bitcast_fusion = (bf16[4,16,256]{2,1,0:T(8,128)(2,1)S(1)}, bf16[4,16,256]{2,1,0:T(8,128)(2,1)S(1)}) fusion(bf16[16,4,256]{2,1,0:T(4,128)(2,1)} %param.24, bf16[16,4,256]{2,1,0:T(4,128)(2,1)} %param.23), kind=kLoop, calls=%fused_computation | loop fusion | bytes 131072 | tf_op jit(solution)/shard_map/transpose | solution.py:167
  8.9 5.1 %state.1 = (f32[16,2,128,128]{3,2,1,0:T(8,128)}, bf16[16,2,128,128]{3,2,1,0:T(8,128)(2,1)S(1)}) custom-call(s32[1,16]{1,0:T(1,128)} %bitcast.26, f32[1,256]{1,0:T(1,128)} %bitcast.20, bf16[4,16,256]{2,1,0:T(8,128)(2,1)S(1)} %get-tuple-element.7.prev_forget, bf16[4,16,256]{2,1,0:T(8,128)(2,1)S(1)} %get-tuple-element.6.prev_input, f32[16,2,128,128]{3,2,1,0:T(8,128)} %base.1), custom_call_target="tpu_custom_call" | custom-call | flops 200000000 | bytes 6000000 | tf_op jit(solution)/shard_map/state/pallas_call | solution.py:149
  14.0 3.0 %all-to-all-done = bf16[128,4,256]{2,1,0:T(4,128)(2,1)S(1)} async-done(((bf16[128,4,256]{2,1,0:T(4,128)(2,1)}), bf16[128,4,256]{2,1,0:T(4,128)(2,1)S(1)}, u32[]{:S(2)}, u32[]{:S(2)}) %all-to-all-start) | async-done | bytes 262176 | tf_op jit(solution)/shard_map/all_to_all | solution.py:143
  17.1 0.0 copy-done.4
  17.1 0.0 copy-done.5
  17.1 0.0 copy-done.2
  17.1 0.0 copy-done.1
  17.1 0.0 copy-done.3
  17.1 0.0 copy-start
  17.1 2.9 %heads.1 = bf16[64,256]{1,0:T(8,128)(2,1)S(1)} custom-call(bf16[8,64,256]{2,1,0:T(8,128)(2,1)S(1)} %bitcast.17, f32[1,2048]{1,0:T(1,128)S(1)} %bitcast.19, bf16[2048,256]{1,0:T(8,128)(2,1)S(1)} %copy-done.1, bf16[2048,256]{1,0:T(8,128)(2,1)S(1)} %copy-done.2, bf16[2048,256]{1,0:T(8,128)(2,1)} %wi.1, bf16[2048,256]{1,0:T(8,128)(2,1)} %wg.1, ...), custom_call_target="tpu_custom_call" | custom-call | flops 300000000 | bytes 6000000 | tf_op jit(solution)/shard_map/heads/pallas_call | solution.py:170
  20.1 5.4 %all-gather = bf16[256,256]{1,0:T(8,128)(2,1)S(1)} all-gather(bf16[64,256]{1,0:T(8,128)(2,1)S(1)} %heads.1), channel_id=2, replica_groups=mesh['kv'=8,'tp'=4] {'tp'}, dimensions={0}, use_global_device_ids=true | all-gather | bytes 163840 | tf_op jit(solution)/shard_map/all_gather | solution.py:189
  25.5 0.0 copy-done
  25.5 0.8 %out.1 = bf16[8,64,256]{2,1,0:T(8,128)(2,1)S(1)} custom-call(bf16[4,64,256]{2,1,0:T(8,128)(2,1)S(1)} %bitcast.18, bf16[1024,2048]{1,0:T(8,128)(2,1)S(1)} %copy-done), custom_call_target="tpu_custom_call" | custom-call | tf_op jit(solution)/shard_map/out/pallas_call | solution.py:190
  26.3 12.8 %all_to_all.10 = bf16[8,64,256]{2,1,0:T(8,128)(2,1)S(1)} all-to-all(bf16[8,64,256]{2,1,0:T(8,128)(2,1)S(1)} %out.1), channel_id=1, replica_groups=mesh['kv'=8,'tp'=4] {'kv'}, dimensions={0} | all-to-all | bytes 524288 | tf_op jit(solution)/shard_map/all_to_all | solution.py:198
  39.2 0.8 %copy.18 = bf16[8,16,4,256]{3,2,1,0:T(4,128)(2,1)} copy(bf16[8,16,4,256]{3,1,2,0:T(8,128)(2,1)S(1)} %bitcast.24) | data formatting | bytes 524288 | tf_op jit(solution)/shard_map/transpose | solution.py:199
  (1 shorter events, 0.0 us)
Async XLA Ops:
  0.6 16.4 %copy-start.4 = (f32[256]{0:T(256)S(1)}, f32[256]{0:T(256)}, u32[]{:S(2)}) copy-start(f32[256]{0:T(256)} %param.20) | copy-start | bytes 3076
  0.6 16.4 %copy-start.5 = (f32[128]{0:T(128)S(1)}, f32[128]{0:T(128)}, u32[]{:S(2)}) copy-start(f32[128]{0:T(128)} %param.21) | copy-start | bytes 1540
  0.7 16.4 %copy-start.2 = (bf16[2048,256]{1,0:T(8,128)(2,1)S(1)}, bf16[2048,256]{1,0:T(8,128)(2,1)}, u32[]{:S(2)}) copy-start(bf16[2048,256]{1,0:T(8,128)(2,1)} %wf.1) | copy-start | bytes 3145732
  0.7 16.4 %copy-start.1 = (bf16[2048,256]{1,0:T(8,128)(2,1)S(1)}, bf16[2048,256]{1,0:T(8,128)(2,1)}, u32[]{:S(2)}) copy-start(bf16[2048,256]{1,0:T(8,128)(2,1)} %wq.1) | copy-start | bytes 3145732
  0.7 16.4 %copy-start.3 = (f32[2048]{0:T(1024)S(1)}, f32[2048]{0:T(1024)}, u32[]{:S(2)}) copy-start(f32[2048]{0:T(1024)} %param.14) | copy-start | bytes 24580
  0.7 16.3 %all-to-all-start = ((bf16[128,4,256]{2,1,0:T(4,128)(2,1)}), bf16[128,4,256]{2,1,0:T(4,128)(2,1)S(1)}, u32[]{:S(2)}, u32[]{:S(2)}) async-start(bf16[128,4,256]{2,1,0:T(4,128)(2,1)} %param.13), calls=%async_computation | async-start | bytes 524288 | tf_op jit(solution)/shard_map/all_to_all | solution.py:143
  17.1 8.4 %copy-start = (bf16[1024,2048]{1,0:T(8,128)(2,1)S(1)}, bf16[1024,2048]{1,0:T(8,128)(2,1)}, u32[]{:S(2)}) copy-start(bf16[1024,2048]{1,0:T(8,128)(2,1)} %w.1) | copy-start | bytes 12582916

commit v2 on v1

--- a/solution.py
+++ b/solution.py
@@ -59,14 +59,12 @@
 
 def heads_kernel(
     n_kv, seqs, props, heads, x, gain, wq, wf, wi, wg, floor, head_gain, low, out,
-    w_sc, s_sc, n_sc, q_sc, o_sc, w_sem, s_sem,
+    w_sc, n_sc, q_sc, o_sc, w_sem,
 ):
     rows = seqs * props
-    loads = [pltpu.make_async_copy(w, w_sc.at[i], w_sem.at[i]) for i, w in enumerate((wf, wq, wi, wg))]
+    loads = [pltpu.make_async_copy(w, w_sc.at[i], w_sem.at[i]) for i, w in enumerate((wi, wg))]
     for c in loads:
         c.start()
-    s_load = pltpu.make_async_copy(low, s_sc, s_sem)
-    s_load.start()
     width = x.shape[2]
     total = jnp.zeros((rows, 1), F32)
     for i in range(n_kv):
@@ -77,14 +75,15 @@
         c = slice(i * width, (i + 1) * width)
         n_sc[:, c] = (x[i].astype(F32) * scale * gain[:, c]).astype(BF16)
 
-    def project(i):
-        loads[i].wait()
-        y = jnp.dot(n_sc[...], w_sc[i], preferred_element_type=F32).astype(BF16).astype(F32)
+    def project(w, load=None):
+        if load is not None:
+            load.wait()
+        y = jnp.dot(n_sc[...], w[...], preferred_element_type=F32).astype(BF16).astype(F32)
         return [y[t * seqs : (t + 1) * seqs, :] for t in range(props)]
 
     fl = floor[...]
-    f = [fl + (1.0 - fl) * jax.nn.sigmoid(y) for y in project(0)]
-    q = [y * jax.nn.sigmoid(y) for y in project(1)]
+    f = [fl + (1.0 - fl) * jax.nn.sigmoid(y) for y in project(wf)]
+    q = [y * jax.nn.sigmoid(y) for y in project(wq)]
     decay = jnp.ones_like(f[0])
     for t in range(props):
         decay = decay * f[t]
@@ -92,14 +91,13 @@
         for h in range(heads):
             at = (h * props + t) * seqs
             q_sc[at : at + seqs, :] = qt[:, h * HEAD_DIM : (h + 1) * HEAD_DIM]
-    v = project(2)
-    s_load.wait()
+    v = project(w_sc.at[0], loads[0])
     for s in range(seqs):
         for h in range(heads):
             each = pl.ds(h * props * seqs + s, props, stride=seqs)
             lhs = q_sc[each, :].astype(BF16)
-            o_sc[each, :] = jnp.dot(lhs, s_sc[s, h], preferred_element_type=F32)
-    g = project(3)
+            o_sc[each, :] = jnp.dot(lhs, low[s, h], preferred_element_type=F32)
+    g = project(w_sc.at[1], loads[1])
     for t in range(props):
         parts = []
         for h in range(heads):
@@ -138,7 +136,7 @@
     rows = seqs * props
     heads = w_query.shape[1] // HEAD_DIM
     own = heads * HEAD_DIM
-    vmem, anym, hbm = (pl.BlockSpec(memory_space=m) for m in (pltpu.VMEM, pl.ANY, pltpu.HBM))
+    vmem, hbm = (pl.BlockSpec(memory_space=m) for m in (pltpu.VMEM, pltpu.HBM))
 
     arrived = lax.all_to_all(hidden, "kv", split_axis=0, concat_axis=0, tiled=True)
     x = arrived.reshape(n_kv, seqs, props, feats).transpose(0, 2, 1, 3).reshape(n_kv, rows, feats)
@@ -170,16 +168,14 @@
     mixed_heads = pl.pallas_call(
         functools.partial(heads_kernel, n_kv, seqs, props, heads),
         out_shape=jax.ShapeDtypeStruct((rows, own), BF16),
-        in_specs=[vmem, vmem, anym, anym, hbm, hbm, vmem, vmem, anym],
+        in_specs=[vmem, vmem, vmem, vmem, hbm, hbm, vmem, vmem, vmem],
         out_specs=vmem,
         scratch_shapes=[
-            pltpu.VMEM((4, n_kv * feats, own), BF16),
-            pltpu.VMEM(state_shape, BF16),
+            pltpu.VMEM((2, n_kv * feats, own), BF16),
             pltpu.VMEM((rows, n_kv * feats), BF16),
             pltpu.VMEM((heads * rows, HEAD_DIM), F32),
             pltpu.VMEM((heads * rows, HEAD_DIM), F32),
-            pltpu.SemaphoreType.DMA((4,)),
-            pltpu.SemaphoreType.DMA,
+            pltpu.SemaphoreType.DMA((2,)),
         ],
         cost_estimate=pl.CostEstimate(flops=300_000_000, bytes_accessed=6_000_000, transcendentals=0),
         compiler_params=pltpu.CompilerParams(vmem_limit_bytes=16 * 2**20),

time: 40.4 us -> 39.8 us (0.985)
  Pallas kernels: 8.88 us -> 8.32 us
    pallas_call x1, Pallas kernels: 2.94 us -> 2.39 us  [shards(): pl.pallas_call(functools.partial(heads_kernel, n_kv, seqs, props, heads),...]
where the time goes in v2:
time: 39.8 us; the launch traced here: 39.4 us
  blocking collectives  18.2 us (46%)
  Pallas kernels  8.32 us (21%)
  starting transfers between devices  7.42 us (19%)
  waiting for transfers between devices  3.02 us (8%)
  local copies, waits for them, and re-layouts  1.68 us (4%)
  between operations  0.75 us (2%)
    all_to_all x1, blocking collectives, shards(): lax.all_to_all(finished, 'kv', split_axis=0, concat_axis=0, tiled=True)  12.8 us
    all_to_all x1, starting transfers between devices, shards(): lax.all_to_all(hidden, 'kv', split_axis=0, concat_axis=0, tiled=True)  7.42 us
    all_gather x1, blocking collectives, shards(): whole = lax.all_gather(mixed_heads, 'tp', axis=0)  5.42 us
    pallas_call x1, Pallas kernels, shards(): pl.pallas_call(functools.partial(state_kernel, seqs, props, heads), out_s...  5.1 us
    all_to_all x1, waiting for transfers between devices, shards(): lax.all_to_all(hidden, 'kv', split_axis=0, concat_axis=0, tiled=True)  3.02 us
    pallas_call x1, Pallas kernels, shards(): pl.pallas_call(functools.partial(heads_kernel, n_kv, seqs, props, heads),...  2.39 us
    transpose x1, local copies, waits for them, and re-layouts, shards(): mixed.reshape(n_kv, props, seqs, feats).transpose(0, 2, 1, 3)  0.84 us
    pallas_call x1, Pallas kernels, shards(): pl.pallas_call(functools.partial(out_kernel, n_tp, n_kv), out_shape=jax.S...  0.83 us
  transfers between devices with their start and end apart: 1, of which 1 were waited for; matrix products, arithmetic and copies ran while one was open for 2% of the time, Pallas kernels for 13%

profile of v2, /device:TPU:0, one launch (start us, length us, event | category | flops | bytes accessed | tf_op | source)
XLA Modules:
  0.0 39.4 jit_solution(7393518883037700174)
XLA Ops:
  0.6 0.0 copy-start.4
  0.6 0.0 copy-start.5
  0.7 0.0 copy-start.2
  0.7 0.0 copy-start.1
  0.7 0.0 copy-start.3
  0.7 7.4 %all-to-all-start = ((bf16[128,4,256]{2,1,0:T(4,128)(2,1)}), bf16[128,4,256]{2,1,0:T(4,128)(2,1)S(1)}, u32[]{:S(2)}, u32[]{:S(2)}) async-start(bf16[128,4,256]{2,1,0:T(4,128)(2,1)} %param.13), calls=%async_computation | async-start | bytes 524288 | tf_op jit(solution)/shard_map/all_to_all | solution.py:141
  8.1 0.8 %copy_bitcast_fusion = (bf16[4,16,256]{2,1,0:T(8,128)(2,1)S(1)}, bf16[4,16,256]{2,1,0:T(8,128)(2,1)S(1)}) fusion(bf16[16,4,256]{2,1,0:T(4,128)(2,1)} %param.24, bf16[16,4,256]{2,1,0:T(4,128)(2,1)} %param.23), kind=kLoop, calls=%fused_computation | loop fusion | bytes 131072 | tf_op jit(solution)/shard_map/transpose | solution.py:165
  8.9 5.1 %state.1 = (f32[16,2,128,128]{3,2,1,0:T(8,128)}, bf16[16,2,128,128]{3,2,1,0:T(8,128)(2,1)S(1)}) custom-call(s32[1,16]{1,0:T(1,128)} %bitcast.26, f32[1,256]{1,0:T(1,128)} %bitcast.20, bf16[4,16,256]{2,1,0:T(8,128)(2,1)S(1)} %get-tuple-element.7.prev_forget, bf16[4,16,256]{2,1,0:T(8,128)(2,1)S(1)} %get-tuple-element.6.prev_input, f32[16,2,128,128]{3,2,1,0:T(8,128)} %base.1), custom_call_target="tpu_custom_call" | custom-call | flops 200000000 | bytes 6000000 | tf_op jit(solution)/shard_map/state/pallas_call | solution.py:147
  14.0 3.0 %all-to-all-done = bf16[128,4,256]{2,1,0:T(4,128)(2,1)S(1)} async-done(((bf16[128,4,256]{2,1,0:T(4,128)(2,1)}), bf16[128,4,256]{2,1,0:T(4,128)(2,1)S(1)}, u32[]{:S(2)}, u32[]{:S(2)}) %all-to-all-start) | async-done | bytes 262176 | tf_op jit(solution)/shard_map/all_to_all | solution.py:141
  17.1 0.0 copy-done.4
  17.1 0.0 copy-done.5
  17.1 0.0 copy-done.2
  17.1 0.0 copy-done.1
  17.1 0.0 copy-done.3
  17.1 0.0 copy-start
  17.1 2.4 %heads.1 = bf16[64,256]{1,0:T(8,128)(2,1)S(1)} custom-call(bf16[8,64,256]{2,1,0:T(8,128)(2,1)S(1)} %bitcast.17, f32[1,2048]{1,0:T(1,128)S(1)} %bitcast.19, bf16[2048,256]{1,0:T(8,128)(2,1)S(1)} %copy-done.1, bf16[2048,256]{1,0:T(8,128)(2,1)S(1)} %copy-done.2, bf16[2048,256]{1,0:T(8,128)(2,1)} %wi.1, bf16[2048,256]{1,0:T(8,128)(2,1)} %wg.1, ...), custom_call_target="tpu_custom_call" | custom-call | flops 300000000 | bytes 6000000 | tf_op jit(solution)/shard_map/heads/pallas_call | solution.py:168
  19.5 5.4 %all-gather = bf16[256,256]{1,0:T(8,128)(2,1)S(1)} all-gather(bf16[64,256]{1,0:T(8,128)(2,1)S(1)} %heads.1), channel_id=2, replica_groups=mesh['kv'=8,'tp'=4] {'tp'}, dimensions={0}, use_global_device_ids=true | all-gather | bytes 163840 | tf_op jit(solution)/shard_map/all_gather | solution.py:185
  24.9 0.0 copy-done
  24.9 0.8 %out.1 = bf16[8,64,256]{2,1,0:T(8,128)(2,1)S(1)} custom-call(bf16[4,64,256]{2,1,0:T(8,128)(2,1)S(1)} %bitcast.18, bf16[1024,2048]{1,0:T(8,128)(2,1)S(1)} %copy-done), custom_call_target="tpu_custom_call" | custom-call | tf_op jit(solution)/shard_map/out/pallas_call | solution.py:186
  25.8 12.8 %all_to_all.10 = bf16[8,64,256]{2,1,0:T(8,128)(2,1)S(1)} all-to-all(bf16[8,64,256]{2,1,0:T(8,128)(2,1)S(1)} %out.1), channel_id=1, replica_groups=mesh['kv'=8,'tp'=4] {'kv'}, dimensions={0} | all-to-all | bytes 524288 | tf_op jit(solution)/shard_map/all_to_all | solution.py:194
  38.6 0.8 %copy.18 = bf16[8,16,4,256]{3,2,1,0:T(4,128)(2,1)} copy(bf16[8,16,4,256]{3,1,2,0:T(8,128)(2,1)S(1)} %bitcast.24) | data formatting | bytes 524288 | tf_op jit(solution)/shard_map/transpose | solution.py:195
  (1 shorter events, 0.0 us)
Async XLA Ops:
  0.6 16.4 %copy-start.4 = (f32[256]{0:T(256)S(1)}, f32[256]{0:T(256)}, u32[]{:S(2)}) copy-start(f32[256]{0:T(256)} %param.20) | copy-start | bytes 3076
  0.6 16.4 %copy-start.5 = (f32[128]{0:T(128)S(1)}, f32[128]{0:T(128)}, u32[]{:S(2)}) copy-start(f32[128]{0:T(128)} %param.21) | copy-start | bytes 1540
  0.7 16.4 %copy-start.2 = (bf16[2048,256]{1,0:T(8,128)(2,1)S(1)}, bf16[2048,256]{1,0:T(8,128)(2,1)}, u32[]{:S(2)}) copy-start(bf16[2048,256]{1,0:T(8,128)(2,1)} %wf.1) | copy-start | bytes 3145732
  0.7 16.4 %copy-start.1 = (bf16[2048,256]{1,0:T(8,128)(2,1)S(1)}, bf16[2048,256]{1,0:T(8,128)(2,1)}, u32[]{:S(2)}) copy-start(bf16[2048,256]{1,0:T(8,128)(2,1)} %wq.1) | copy-start | bytes 3145732
  0.7 16.4 %copy-start.3 = (f32[2048]{0:T(1024)S(1)}, f32[2048]{0:T(1024)}, u32[]{:S(2)}) copy-start(f32[2048]{0:T(1024)} %param.14) | copy-start | bytes 24580
  0.7 16.3 %all-to-all-start = ((bf16[128,4,256]{2,1,0:T(4,128)(2,1)}), bf16[128,4,256]{2,1,0:T(4,128)(2,1)S(1)}, u32[]{:S(2)}, u32[]{:S(2)}) async-start(bf16[128,4,256]{2,1,0:T(4,128)(2,1)} %param.13), calls=%async_computation | async-start | bytes 524288 | tf_op jit(solution)/shard_map/all_to_all | solution.py:141
  17.1 7.8 %copy-start = (bf16[1024,2048]{1,0:T(8,128)(2,1)S(1)}, bf16[1024,2048]{1,0:T(8,128)(2,1)}, u32[]{:S(2)}) copy-start(bf16[1024,2048]{1,0:T(8,128)(2,1)} %w.1) | copy-start | bytes 12582916
